TPU v7x, 32 devices: a whole 2x2x4 slice. The times are simulated.
32 devices in a mesh: ep: 8 (over z, core), tp: 4 (over y, x).
Axes of the slice: x: 2, y: 2, z: 4, core: 2. Of those that a mesh axis runs over, the one named last changes fastest.
Arguments:
- queries: bfloat16 [2048, 4096], P('ep', 'tp'), may hold values from -6 to 6
- keys: bfloat16 [2048, 1024], P('ep', 'tp'), may hold values from -6 to 6
- values: bfloat16 [2048, 1024], P('ep', 'tp'), may hold values from -6 to 6
- query_gain: float32 [64], replicated, may hold values from 1 to 11
- key_gain: float32 [64], replicated, may hold values from 1 to 11
- moe_rows: bfloat16 [2048, 4096], P('ep', 'tp'), may hold values from -14 to 14
- route_ids: int32 [2048, 2], P('ep'), may hold values from 0 to 7, all different within a row; in each aligned block of 256 rows (0 to 255, 256 to 511, ...) at most 96 rows name the same one
- group_weight: float32 [2048], P('ep'), may hold values from 0.2 to 1
- expert_weight: float32 [2048, 2], P('ep'), may hold values from 0.05 to 1
- expert_gate: bfloat16 [8, 4096, 2048], P('ep', None, 'tp'), may hold values from -0.09375 to 0.09375
- expert_up: bfloat16 [8, 4096, 2048], P('ep', None, 'tp'), may hold values from -0.09375 to 0.09375
- expert_down: bfloat16 [8, 2048, 4096], P('ep', None, 'tp'), may hold values from -0.125 to 0.125
Outputs:
- attended: bfloat16 [2048, 4096], P('ep', 'tp')
- moe_out: bfloat16 [2048, 4096], P('ep', 'tp')
Inputs may be any that keep to these rules, and one draw needn't show every extreme that they name: `route_ids`: each row names 2 different experts. Among the rows of one device no expert is named by more than 96 rows, and in every draw some expert is named by exactly 96 of them.
All inputs are finite; a program needn't handle non-finite values.
Results may differ from a plain program's by a relative error of at most 0.0055.
The roundings to bfloat16 on the way count: a program that leaves them out, or rounds other values in their place, can miss the bound.
Values may be sent and summed in bfloat16 or wider, within the bound.
A program may use at most 128 MiB of HBM per device.

v0:
```python
import jax
import jax.numpy as jnp
from jax import lax
from jax.sharding import PartitionSpec as P

D = 4096
HEAD_DIM = 64
GRID_W = 64
TOPK = 2


def rotary_tables(position):
    pair_count = HEAD_DIM // 4
    grid_pos = jnp.stack([position // GRID_W, position % GRID_W], axis=-1).astype(jnp.float32)
    frequency = 10000.0 ** (-jnp.arange(pair_count, dtype=jnp.float32) / pair_count)
    angles = grid_pos[:, :, None] * frequency
    return (jnp.cos(angles), jnp.sin(angles))


def normed_rotated(rows_in, gain, cosine, sine_of):
    row_count, head_count = (rows_in.shape[0], rows_in.shape[1])
    pair_count = HEAD_DIM // 4
    scaled = rows_in * lax.rsqrt(jnp.mean(rows_in * rows_in, axis=-1, keepdims=True) + 1e-06) * gain
    parted = scaled.reshape(row_count, head_count, 2, 2, pair_count)
    first_half, second = (parted[:, :, :, 0, :], parted[:, :, :, 1, :])
    cos_b, sin_b = (cosine[:, None], sine_of[:, None])
    turned = jnp.stack(
        [first_half * cos_b - second * sin_b, second * cos_b + first_half * sin_b], axis=3
    )
    return turned.reshape(row_count, head_count, HEAD_DIM).astype(jnp.bfloat16)


def attend_block(carried, portion, query_rot, kv_width):
    running_max, denominator, summed = carried
    key_count = portion.shape[0]
    head_count = kv_width // HEAD_DIM
    keys_part = portion[:, :kv_width].reshape(key_count, head_count, HEAD_DIM)
    values_part = portion[:, kv_width:].reshape(key_count, head_count, HEAD_DIM)
    scores = jnp.einsum(
        "tkgd,skd->kgts", query_rot, keys_part, preferred_element_type=jnp.float32
    ) * HEAD_DIM ** (-0.5)
    new_max = jnp.max(scores, axis=-1)
    factor = jnp.exp(running_max - new_max)
    weights = jnp.exp(scores - new_max[..., None])
    denominator = denominator * factor + jnp.sum(weights, axis=-1)
    summed = summed * factor[..., None] + jnp.einsum(
        "kgts,skd->kgtd",
        weights.astype(jnp.bfloat16),
        values_part,
        preferred_element_type=jnp.float32,
    )
    return (new_max, denominator, summed)


def on_device(
    queries,
    keys,
    values,
    query_gain,
    key_gain,
    moe_rows,
    route_ids,
    group_weight,
    expert_weight,
    expert_gate,
    expert_up,
    expert_down,
):
    tok_rows = queries.shape[0]
    q_heads = queries.shape[1] // HEAD_DIM
    k_heads = keys.shape[1] // HEAD_DIM
    group_size = q_heads // k_heads
    position = lax.axis_index("ep") * tok_rows + jnp.arange(tok_rows, dtype=jnp.int32)
    cosine, sine_of = rotary_tables(position)
    query_rot = normed_rotated(
        queries.astype(jnp.float32).reshape(tok_rows, q_heads, HEAD_DIM),
        query_gain,
        cosine,
        sine_of,
    )
    query_rot = query_rot.reshape(tok_rows, k_heads, group_size, HEAD_DIM)
    key_rot = normed_rotated(
        keys.astype(jnp.float32).reshape(tok_rows, k_heads, HEAD_DIM), key_gain, cosine, sine_of
    )
    kv_width = k_heads * HEAD_DIM
    joined = jnp.concatenate([key_rot.reshape(tok_rows, kv_width), values], axis=1)
    initial = (
        jnp.full((k_heads, group_size, tok_rows), -jnp.inf, jnp.float32),
        jnp.zeros((k_heads, group_size, tok_rows), jnp.float32),
        jnp.zeros((k_heads, group_size, tok_rows, HEAD_DIM), jnp.float32),
    )
    final_max, denominator, summed = attend_block(
        initial, lax.all_gather(joined, "ep", axis=0, tiled=True), query_rot, kv_width
    )
    attended = (
        (summed / denominator[..., None])
        .transpose(2, 0, 1, 3)
        .reshape(tok_rows, q_heads * HEAD_DIM)
        .astype(jnp.bfloat16)
    )
    moe_tokens = moe_rows.shape[0]
    local_experts = expert_gate.shape[0]
    expert_count = local_experts * lax.axis_size("ep")
    capacity = 3 * moe_tokens * TOPK // (2 * expert_count)
    picks = moe_tokens * TOPK
    route_list = route_ids.reshape(picks)
    one_hot = (route_list[:, None] == jnp.arange(expert_count, dtype=jnp.int32)[None, :]).astype(
        jnp.int32
    )
    rank_of = jnp.sum((jnp.cumsum(one_hot, axis=0) - one_hot) * one_hot, axis=1)
    slot_of = route_list * capacity + rank_of
    owner_of = (
        jnp.full((expert_count * capacity,), moe_tokens, jnp.int32)
        .at[slot_of]
        .set(jnp.arange(picks, dtype=jnp.int32) // TOPK)
    )
    padded = jnp.concatenate([moe_rows, jnp.zeros((1, moe_rows.shape[1]), moe_rows.dtype)], axis=0)
    arrived = lax.all_to_all(
        padded[owner_of].reshape(expert_count, capacity, moe_rows.shape[1]),
        "ep",
        split_axis=0,
        concat_axis=1,
        tiled=True,
    )
    portion = lax.all_gather(arrived, "tp", axis=2, tiled=True)
    widened = portion.astype(jnp.float32)
    gate_act = jnp.einsum("erd,edf->erf", portion, expert_gate, preferred_element_type=jnp.float32)
    up_act = jnp.einsum("erd,edf->erf", portion, expert_up, preferred_element_type=jnp.float32)
    square_sum = jnp.sum(widened * widened, axis=2)
    inv_rms = lax.rsqrt(square_sum / D + 1e-06)[..., None]
    hidden = (jax.nn.silu(gate_act * inv_rms) * (up_act * inv_rms)).astype(jnp.bfloat16)
    out_cols = expert_down.shape[2]
    expert_result = jnp.einsum(
        "erf,efd->erd",
        lax.all_gather(hidden, "tp", axis=2, tiled=True),
        expert_down,
        preferred_element_type=jnp.float32,
    ).astype(jnp.bfloat16)
    returned = lax.all_to_all(expert_result, "ep", split_axis=1, concat_axis=0, tiled=True)
    flat_back = returned.reshape(expert_count * capacity, out_cols)
    picked = flat_back[slot_of].reshape(moe_tokens, TOPK, out_cols).astype(jnp.float32)
    mixing = group_weight[:, None] * expert_weight / jnp.sum(expert_weight, axis=1, keepdims=True)
    moe_out = jnp.sum(mixing[:, :, None] * picked, axis=1).astype(jnp.bfloat16)
    return (attended, moe_out)


def solution(mesh):
    placed = (
        P("ep", "tp"),
        P("ep", "tp"),
        P("ep", "tp"),
        P(),
        P(),
        P("ep", "tp"),
        P("ep", None),
        P("ep"),
        P("ep", None),
        P("ep", None, "tp"),
        P("ep", None, "tp"),
        P("ep", None, "tp"),
    )
    return jax.shard_map(
        on_device,
        mesh=mesh,
        in_specs=placed,
        out_specs=(P("ep", "tp"), P("ep", "tp")),
        check_vma=False,
    )
```

profile of v0, /device:TPU:0, one launch (start us, length us, event | category | flops | bytes accessed | tf_op | source)
XLA Modules:
  0.0 295.3 jit_solution(2823822702659321500)
XLA Ops:
  7.2 0.0 all-gather.7.cloned.1.call-start
  7.2 0.7 broadcast_multiply_fusion
  7.9 0.8 copy.47
  8.7 0.1 eq.31
  8.9 0.1 eq.27
  9.0 0.1 copy.46
  9.2 0.1 mul.255
  9.3 1.1 reduce-window.6
  10.5 0.2 slice_reduce_fusion
  10.7 0.1 fusion.36
  10.8 2.4 scatter_custom_fusion
  13.3 1.1 concatenate.11
  14.4 2.8 gather_fusion
  17.2 0.0 copy-start.3
  17.2 0.0 copy-start.7
  17.2 0.0 copy-start.4
  17.2 44.2 %all_to_all.21 = bf16[8,96,1024]{2,1,0:T(8,128)(2,1)} all-to-all(bf16[8,96,1024]{2,1,0:T(8,128)(2,1)S(1)} %bitcast.104), channel_id=1, replica_groups=mesh['ep'=8,'tp'=4] {'ep'}, dimensions={0} | all-to-all | bytes 3145728 | tf_op jit(solution)/shard_map/all_to_all | solution.py:118
  61.4 0.0 all-gather.7.cloned.1.call-update
  61.5 0.0 all-gather.5.cloned.1.call-start
  61.5 0.1 copy.42
  61.6 0.1 mul.220
  61.7 0.1 copy.41
  61.9 0.2 multiply_cosine_fusion
  62.1 0.1 multiply_multiply_fusion.1
  62.3 0.7 pad_maximum_fusion.1
  63.0 0.0 all-gather.5.cloned.1.call-update
  63.1 0.5 all-gather.9.cloned.1.call-start
  63.6 67.0 %all-gather.7.cloned.1.call-done = bf16[1,768,4096]{2,1,0:T(8,128)(2,1)} async-done(((bf16[1,768,1024]{2,1,0:T(8,128)(2,1)}), bf16[1,768,4096]{2,1,0:T(8,128)(2,1)}) %all-gather.7.cloned.1.call-update) | async-done | bytes 6291472 | tf_op jit(solution)/shard_map/all_gather | solution.py:125
  130.6 4.2 %multiply_reduce_fusion = f32[768]{0:T(1024)S(1)} fusion(bf16[1,768,4096]{2,1,0:T(8,128)(2,1)} %all-gather.7.cloned.1.call-done), kind=kLoop, calls=%fused_computation.9 | loop fusion | flops 9436416 | bytes 6294528 | tf_op jit(solution)/shard_map/reduce_sum | solution.py:129
  134.8 0.4 copy-done
  135.2 5.5 %fusion.5 = f32[768,512]{1,0:T(8,128)S(1)} fusion(bf16[1,768,4096]{2,1,0:T(8,128)(2,1)S(1)} %copy-done, bf16[1,4096,512]{2,1,0:T(8,128)(2,1)} %param.22), kind=kOutput, calls=%fused_computation.10 | convolution fusion | flops 3221225472 | bytes 12058624 | tf_op jit(solution)/shard_map/erd,edf->erf/dot_general | solution.py:128
  140.7 0.0 copy-start.8
  140.7 0.0 copy-start.2
  140.8 0.0 copy-start.5
  140.8 0.0 copy-start.6
  140.8 4.6 %multiply_convert_fusion = bf16[768,512]{1,0:T(8,128)(2,1)} fusion(f32[768,512]{1,0:T(8,128)S(1)} %fusion.5, bf16[1,4096,512]{2,1,0:T(8,128)(2,1)S(1)} %copy-done.9, bf16[1,768,4096]{2,1,0:T(8,128)(2,1)S(1)} %copy-done, f32[768]{0:T(1024)S(1)} %add_rsqrt_fusion.1), kind=kOutput, calls=%fused_computation.21 | convolution fusion | flops 3224371200 | bytes 12848128 | tf_op jit(solution)/shard_map/erd,edf->erf/dot_general | solution.py:127
  145.4 0.0 all-gather.9.cloned.1.call-update
  145.4 0.1 mul.237
  145.5 0.0 copy-done.2
  145.5 0.2 copy.43
  145.7 0.0 copy-done.5
  145.8 0.1 copy.45
  145.9 0.1 bitcast_reduce_fusion.1
  146.1 0.2 multiply_multiply_fusion
  146.3 0.2 subtract_convert_fusion
  146.5 16.9 %all-gather.5.cloned.1.call-done = bf16[2048,512]{0,1:T(8,128)(2,1)} async-done(((bf16[256,512]{0,1:T(8,128)(2,1)}), bf16[2048,512]{0,1:T(8,128)(2,1)}) %all-gather.5.cloned.1.call-update) | async-done | bytes 2097168 | tf_op jit(solution)/shard_map/all_gather | solution.py:93
  163.4 2.7 fusion.44
  166.1 13.9 %bitcast_reduce_fusion = (f32[4,4,256]{2,1,0:T(4,128)S(1)}, f32[4,2048,256,4]{2,1,3,0:T(8,128)}) fusion(bf16[2048,4,64,1]{0,2,3,1:T(8,128)(2,1)S(1)} %bitcast.107, bf16[256,4,4,64]{0,3,2,1:T(8,128)(2,1)S(1)} %bitcast.108), kind=kOutput, calls=%fused_computation.4 | convolution fusion | flops 1090514944 | bytes 35143680 | tf_op jit(solution)/shard_map/tkgd,skd->kgts/dot_general | solution.py:39
  180.1 27.9 %all-gather.9.cloned.1.call-done = bf16[768,2048]{1,0:T(8,128)(2,1)} async-done(((bf16[768,512]{1,0:T(8,128)(2,1)}), bf16[768,2048]{1,0:T(8,128)(2,1)}) %all-gather.9.cloned.1.call-update) | async-done | bytes 3145744 | tf_op jit(solution)/shard_map/all_gather | solution.py:135
  208.0 6.6 %fusion.16 = bf16[1,768,1024]{2,1,0:T(8,128)(2,1)S(1)} fusion(bf16[768,2048]{1,0:T(8,128)(2,1)} %all-gather.9.cloned.1.call-done, bf16[1,2048,1024]{2,1,0:T(8,128)(2,1)} %param.23), kind=kOutput, calls=%fused_computation.22 | convolution fusion | flops 3222011904 | bytes 8912896 | tf_op jit(solution)/shard_map/erf,efd->erd/dot_general | solution.py:133
  214.5 2.4 copy.58
  217.0 0.5 broadcast.321
  217.5 11.2 %reduce.3 = bf16[768,1024]{1,0:T(8,128)(2,1)} reduce(bf16[768,1,1024]{2,1,0:T(2,128)(2,1)S(1)} %bitcast.101, bf16[]{:T(256)} %broadcast.321), dimensions={1}, to_apply=%bitcast.99.reduce_sub_computation | reduce | bytes 3145730
  228.7 4.1 %reshape.311 = bf16[8,2,49152]{2,1,0:T(2,128)(2,1)} reshape(bf16[768,1024]{1,0:T(8,128)(2,1)} %reduce.3) | data formatting | bytes 3145728
  232.8 4.6 %all-to-all-start.1 = ((bf16[8,2,49152]{2,1,0:T(2,128)(2,1)}), bf16[8,2,49152]{2,1,0:T(2,128)(2,1)S(1)}, u32[]{:S(2)}, u32[]{:S(2)}) async-start(bf16[8,2,49152]{2,1,0:T(2,128)(2,1)} %reshape.311), calls=%async_computation.1 | async-start | bytes 3145728 | tf_op jit(solution)/shard_map/all_to_all | solution.py:139
  237.4 13.6 %fusion.1 = f32[4,4,256]{2,1,0:T(4,128)S(1)} fusion(f32[4,2048,256,4]{2,1,3,0:T(8,128)} %get-tuple-element.19, f32[4,4,256]{2,1,0:T(4,128)S(1)} %get-tuple-element.18), kind=kLoop, calls=%fused_computation.6 | loop fusion | flops 25161728 | bytes 33587200 | tf_op jit(solution)/shard_map/reduce_sum | solution.py:45
  251.1 13.6 %fusion.32 = bf16[256,4,4,64]{0,3,2,1:T(8,128)(2,1)S(1)} fusion(bf16[2048,4,64,1]{0,2,3,1:T(8,128)(2,1)S(1)} %bitcast.106, f32[4,2048,256,4]{2,1,3,0:T(8,128)} %get-tuple-element.19, f32[4,4,256]{2,1,0:T(4,128)S(1)} %get-tuple-element.18, f32[256,4,4]{0,2,1:T(4,128)S(1)} %bitcast_add_fusion, f32[256,4,4]{0,2,1:T(4,128)S(1)} %multiply_bitcast_fusion), kind=kOutput, calls=%fused_computation.26 | convolution fusion | flops 1099694080 | bytes 35176448 | tf_op jit(solution)/shard_map/kgts,skd->kgtd/dot_general | solution.py:46
  264.7 1.0 copy.50
  265.7 9.5 %all-to-all-done.1 = bf16[8,2,49152]{2,1,0:T(2,128)(2,1)S(1)} async-done(((bf16[8,2,49152]{2,1,0:T(2,128)(2,1)}), bf16[8,2,49152]{2,1,0:T(2,128)(2,1)S(1)}, u32[]{:S(2)}, u32[]{:S(2)}) %all-to-all-start.1) | async-done | bytes 1572896 | tf_op jit(solution)/shard_map/all_to_all | solution.py:139
  275.2 3.9 %reshape.312 = bf16[768,1,1024]{2,1,0:T(2,128)(2,1)} reshape(bf16[8,2,49152]{2,1,0:T(2,128)(2,1)S(1)} %all-to-all-done.1) | data formatting | bytes 3145728
  279.1 2.5 copy.57
  281.6 2.1 gather_fusion.1
  283.7 1.3 reshape.278
  285.0 3.5 %multiply_reduce_fusion.1 = bf16[256,1024]{1,0:T(8,128)(2,1)} fusion(f32[256,2,1024]{2,1,0:T(2,128)S(1)} %reshape.278, f32[256,2]{1,0:T(8,128)S(1)} %copy.45), kind=kLoop, calls=%fused_computation.18 | loop fusion | flops 786432 | bytes 2623488 | tf_op jit(solution)/shard_map/reduce_sum | solution.py:143
  (32 shorter events, 0.4 us)
Async XLA Ops:
  7.2 123.4 %all-gather.7.cloned.1.call-start = ((), (), s32[]{:S(2)}) async-start(), calls=%async_computation.3 | async-start | bytes 7864320 | tf_op jit(solution)/shard_map/all_gather | solution.py:125
  17.2 44.3 %copy-start.3 = (bf16[256,256]{1,0:T(8,128)(2,1)S(1)}, bf16[256,256]{1,0:T(8,128)(2,1)}, u32[]{:S(2)}) copy-start(bf16[256,256]{1,0:T(8,128)(2,1)} %param.14) | copy-start | bytes 393220
  17.2 44.4 %copy-start.7 = (f32[64]{0:T(128)S(1)}, f32[64]{0:T(128)}, u32[]{:S(2)}) copy-start(f32[64]{0:T(128)} %param.16) | copy-start | bytes 772
  17.2 44.5 %copy-start.4 = (bf16[256,256]{1,0:T(8,128)(2,1)S(1)}, bf16[256,256]{1,0:T(8,128)(2,1)}, u32[]{:S(2)}) copy-start(bf16[256,256]{1,0:T(8,128)(2,1)} %param.13) | copy-start | bytes 393220
  61.5 101.9 %all-gather.5.cloned.1.call-start = ((), (), s32[]{:S(2)}) async-start(), calls=%async_computation.2 | async-start | bytes 2359296 | tf_op jit(solution)/shard_map/all_gather | solution.py:93
  63.1 144.9 %all-gather.9.cloned.1.call-start = ((), (), s32[]{:S(2)}) async-start(), calls=%async_computation.4 | async-start | bytes 3932160 | tf_op jit(solution)/shard_map/all_gather | solution.py:135
  130.6 4.6 %copy-start = (bf16[1,768,4096]{2,1,0:T(8,128)(2,1)S(1)}, bf16[1,768,4096]{2,1,0:T(8,128)(2,1)}, u32[]{:S(2)}) copy-start(bf16[1,768,4096]{2,1,0:T(8,128)(2,1)} %all-gather.7.cloned.1.call-done) | copy-start | bytes 18874372
  135.2 5.5 %copy-start.9 = (bf16[1,4096,512]{2,1,0:T(8,128)(2,1)S(1)}, bf16[1,4096,512]{2,1,0:T(8,128)(2,1)}, u32[]{:S(2)}) copy-start(bf16[1,4096,512]{2,1,0:T(8,128)(2,1)} %param.21) | copy-start | bytes 12582916
  140.7 4.7 %copy-start.8 = (f32[64]{0:T(128)S(1)}, f32[64]{0:T(128)}, u32[]{:S(2)}) copy-start(f32[64]{0:T(128)} %param.15) | copy-start | bytes 772
  140.7 4.8 %copy-start.2 = (bf16[256,1024]{1,0:T(8,128)(2,1)S(1)}, bf16[256,1024]{1,0:T(8,128)(2,1)}, u32[]{:S(2)}) copy-start(bf16[256,1024]{1,0:T(8,128)(2,1)} %param.12) | copy-start | bytes 1572868
  140.8 5.0 %copy-start.5 = (f32[256,2]{0,1:T(2,128)S(1)}, f32[256,2]{0,1:T(2,128)}, u32[]{:S(2)}) copy-start(f32[256,2]{0,1:T(2,128)} %param.20) | copy-start | bytes 6148
  140.8 5.0 %copy-start.6 = (f32[256]{0:T(256)S(1)}, f32[256]{0:T(256)}, u32[]{:S(2)}) copy-start(f32[256]{0:T(256)} %param.19) | copy-start | bytes 3076
  232.8 42.4 %all-to-all-start.1 = ((bf16[8,2,49152]{2,1,0:T(2,128)(2,1)}), bf16[8,2,49152]{2,1,0:T(2,128)(2,1)S(1)}, u32[]{:S(2)}, u32[]{:S(2)}) async-start(bf16[8,2,49152]{2,1,0:T(2,128)(2,1)} %reshape.311), calls=%async_computation.1 | async-start | bytes 3145728 | tf_op jit(solution)/shard_map/all_to_all | solution.py:139
  237.4 13.7 %copy-start.1 = (bf16[2048,256]{0,1:T(8,128)(2,1)S(1)}, bf16[2048,256]{0,1:T(8,128)(2,1)}, u32[]{:S(2)}) copy-start(bf16[2048,256]{0,1:T(8,128)(2,1)} %get-tuple-element.11) | copy-start | bytes 3145732
Sparse Core Ops, SparseCore 0:
  61.6 68.9 all-gather.6
  132.7 30.5 all-gather.4
  165.2 42.7 all-gather.8
where the time goes:
time: 299 us; the launch traced here: 295 us
  waiting for transfers between devices  121 us (40%)
  blocking collectives  44.2 us (15%)
  matrix products  44.2 us (15%)
  other arithmetic  36.3 us (12%)
  local copies, waits for them, and re-layouts  29.7 us (10%)
  between operations  14.4 us (5%)
  starting transfers between devices  5.19 us (2%)
    all_gather x1, waiting for transfers between devices, on_device(): portion = lax.all_gather(arrived, 'tp', axis=2, tiled=True)  67 us
    all_to_all x1, blocking collectives, on_device(): lax.all_to_all(padded[owner_of].reshape(expert_count, capacity, moe_rows....  44.2 us
    all_gather x1, waiting for transfers between devices, on_device(): lax.all_gather(hidden, 'tp', axis=2, tiled=True)  27.9 us
    all_gather x1, waiting for transfers between devices, on_device(): lax.all_gather(joined, 'ep', axis=0, tiled=True)  16.9 us
    dot_general x1, matrix products, attend_block(): jnp.einsum('tkgd,skd->kgts', query_rot, keys_part, preferred_element_type...  13.9 us
    unnamed x29, local copies, waits for them, and re-layouts  13.7 us
    reduce_sum x1, other arithmetic, attend_block(): denominator = denominator * factor + jnp.sum(weights, axis=-1)  13.6 us
    dot_general x1, matrix products, attend_block(): jnp.einsum('kgts,skd->kgtd', weights.astype(jnp.bfloat16), values_part, p...  13.6 us
  transfers between devices with their start and end apart: 4, of which 4 were waited for; matrix products, arithmetic and copies ran while one was open for 21% of the time, Pallas kernels for 0%

commit v1 on v0

--- a/solution.py
+++ b/solution.py
@@ -7,6 +7,16 @@
 HEAD_DIM = 64
 GRID_W = 64
 TOPK = 2
+
+
+def pass_along(value, name, dim):
+    devices = lax.axis_size(name)
+    held, blocks = (value, [value])
+    for _ in range(devices - 1):
+        held = lax.ppermute(held, name, [(i, (i + 1) % devices) for i in range(devices)])
+        blocks.insert(0, held)
+    row_of_blocks = jnp.concatenate(blocks, axis=dim)
+    return jnp.roll(row_of_blocks, (lax.axis_index(name) + 1) * value.shape[dim], axis=dim)
 
 
 def rotary_tables(position):
@@ -122,7 +132,7 @@
         concat_axis=1,
         tiled=True,
     )
-    portion = lax.all_gather(arrived, "tp", axis=2, tiled=True)
+    portion = pass_along(arrived, "tp", 2)
     widened = portion.astype(jnp.float32)
     gate_act = jnp.einsum("erd,edf->erf", portion, expert_gate, preferred_element_type=jnp.float32)
     up_act = jnp.einsum("erd,edf->erf", portion, expert_up, preferred_element_type=jnp.float32)

time: 299 us -> 321 us (1.074)
  waiting for transfers between devices: 121 us -> 139 us
  local copies, waits for them, and re-layouts: 29.7 us -> 37.5 us
    ppermute x0 -> x3, waiting for transfers between devices: none -> 103 us  [pass_along(): lax.ppermute(held, name, [(i, (i + 1) % devices) for i in range(devices)])]
    all_gather x1 -> x0, waiting for transfers between devices: 67 us -> none  [on_device(): portion = lax.all_gather(arrived, 'tp', axis=2, tiled=True)]
    all_gather x1, waiting for transfers between devices: 16.9 us -> 0.02 us  [on_device(): lax.all_gather(joined, 'ep', axis=0, tiled=True)]
    unnamed x29 -> x34, local copies, waits for them, and re-layouts: 13.7 us -> 20.7 us
  transfers between devices with their start and end apart: 4 -> 6, of which waited for: 4 -> 5; matrix products, arithmetic and copies ran while one was open for 21% -> 20% of each run, Pallas kernels for 0% -> 0%
where the time goes in v1:
time: 321 us; the launch traced here: 317 us
  waiting for transfers between devices  139 us (43%)
  blocking collectives  43.9 us (14%)
  matrix products  41.8 us (13%)
  local copies, waits for them, and re-layouts  37.5 us (12%)
  other arithmetic  33.3 us (10%)
  between operations  14.7 us (5%)
  starting transfers between devices  7.23 us (2%)
    ppermute x3, waiting for transfers between devices, pass_along(): lax.ppermute(held, name, [(i, (i + 1) % devices) for i in range(devices)])  103 us
    all_to_all x1, blocking collectives, on_device(): lax.all_to_all(padded[owner_of].reshape(expert_count, capacity, moe_rows....  43.9 us
    all_gather x1, waiting for transfers between devices, on_device(): lax.all_gather(hidden, 'tp', axis=2, tiled=True)  26.1 us
    unnamed x34, local copies, waits for them, and re-layouts  20.7 us
    dot_general x1, matrix products, attend_block(): jnp.einsum('tkgd,skd->kgts', query_rot, keys_part, preferred_element_type...  13.7 us
    reduce_sum x1, other arithmetic, attend_block(): denominator = denominator * factor + jnp.sum(weights, axis=-1)  13.6 us
    dot_general x1, matrix products, attend_block(): jnp.einsum('kgts,skd->kgtd', weights.astype(jnp.bfloat16), values_part, p...  13.6 us
    unnamed x1, other arithmetic  11.2 us
  transfers between devices with their start and end apart: 6, of which 5 were waited for; matrix products, arithmetic and copies ran while one was open for 20% of the time, Pallas kernels for 0%

profile of v1, /device:TPU:0, one launch (start us, length us, event | category | flops | bytes accessed | tf_op | source)
XLA Modules:
  0.0 317.3 jit_solution(8280913886059957763)
XLA Ops:
  7.2 0.0 all-gather.4.cloned.1.call-start
  7.2 0.7 broadcast_multiply_fusion
  7.9 0.8 copy.47
  8.7 0.1 eq.34
  8.9 0.1 eq.30
  9.0 0.1 copy.46
  9.2 0.1 mul.258
  9.3 1.1 reduce-window.6
  10.5 0.2 slice_reduce_fusion
  10.7 0.1 fusion.38
  10.8 2.4 scatter_custom_fusion
  13.3 1.1 concatenate.17
  14.4 2.8 gather_fusion
  17.2 43.9 %all_to_all.21 = bf16[8,96,1024]{2,1,0:T(8,128)(2,1)S(1)} all-to-all(bf16[8,96,1024]{2,1,0:T(8,128)(2,1)S(1)} %bitcast.110), channel_id=1, replica_groups=mesh['ep'=8,'tp'=4] {'ep'}, dimensions={0} | all-to-all | bytes 3145728 | tf_op jit(solution)/shard_map/all_to_all | solution.py:128
  61.2 1.5 collective-permute-start
  62.7 35.2 %collective-permute-done = bf16[1,768,1024]{2,1,0:T(8,128)(2,1)S(1)} collective-permute-done((bf16[1,768,1024]{2,1,0:T(8,128)(2,1)S(1)}, bf16[1,768,1024]{2,1,0:T(8,128)(2,1)S(1)}, u32[]{:S(2)}, u32[]{:S(2)}) %collective-permute-start) | collective-permute-done | bytes 1572896 | tf_op jit(solution)/shard_map/ppermute | solution.py:16
  97.8 0.6 collective-permute-start.1
  98.5 35.3 %collective-permute-done.1 = bf16[1,768,1024]{2,1,0:T(8,128)(2,1)} collective-permute-done((bf16[1,768,1024]{2,1,0:T(8,128)(2,1)S(1)}, bf16[1,768,1024]{2,1,0:T(8,128)(2,1)}, u32[]{:S(2)}, u32[]{:S(2)}) %collective-permute-start.1) | collective-permute-done | bytes 1572896 | tf_op jit(solution)/shard_map/ppermute | solution.py:16
  133.8 0.1 copy.42
  133.9 0.7 mul.223
  134.6 0.1 copy.41
  134.8 0.2 multiply_cosine_fusion
  135.0 0.1 multiply_multiply_fusion.1
  135.2 0.7 pad_maximum_fusion.1
  135.9 0.5 all-gather.6.cloned.1.call-start
  136.4 32.6 %collective-permute-done.2 = bf16[1,768,1024]{2,1,0:T(8,128)(2,1)} collective-permute-done((bf16[1,768,1024]{2,1,0:T(8,128)(2,1)}, bf16[1,768,1024]{2,1,0:T(8,128)(2,1)}, u32[]{:S(2)}, u32[]{:S(2)}) %collective-permute-start.2) | collective-permute-done | bytes 1572896 | tf_op jit(solution)/shard_map/ppermute | solution.py:16
  169.0 1.6 constant_dynamic-update-slice_fusion.7
  170.6 1.6 constant_dynamic-update-slice_fusion.6
  172.2 0.2 constant_dynamic-update-slice_fusion.5
  172.3 0.2 constant_dynamic-update-slice_fusion.4
  172.5 1.6 constant_dynamic-update-slice_fusion.3
  174.1 1.6 constant_dynamic-update-slice_fusion.2
  175.6 0.2 constant_dynamic-update-slice_fusion.1
  175.8 0.2 constant_dynamic-update-slice_fusion
  176.0 1.3 multiply_reduce_fusion
  177.3 0.7 copy-done.7
  178.0 3.4 %fusion.7 = f32[768,512]{1,0:T(8,128)S(1)} fusion(bf16[1,768,8192]{2,1,0:T(8,128)(2,1)S(1)} %constant_dynamic-update-slice_fusion, s32[]{:T(128)S(6)} %select_n.67, bf16[1,4096,512]{2,1,0:T(8,128)(2,1)S(1)} %copy-done.7), kind=kOutput, calls=%fused_computation.12 | convolution fusion | flops 3221225472 | bytes 12058628 | tf_op jit(solution)/shard_map/erd,edf->erf/dot_general | solution.py:137
  181.5 4.5 %multiply_convert_fusion = bf16[768,512]{1,0:T(8,128)(2,1)} fusion(f32[768,512]{1,0:T(8,128)S(1)} %fusion.7, bf16[1,4096,512]{2,1,0:T(8,128)(2,1)S(1)} %copy-done.8, bf16[1,768,8192]{2,1,0:T(8,128)(2,1)S(1)} %constant_dynamic-update-slice_fusion, s32[]{:T(128)S(6)} %select_n.67, f32[768]{0:T(1024)S(1)} %add_rsqrt_fusion.1), kind=kOutput, calls=%fused_computation.23 | convolution fusion | flops 3224371200 | bytes 12849156 | tf_op jit(solution)/shard_map/erd,edf->erf/dot_general | solution.py:138
  186.0 0.0 all-gather.6.cloned.1.call-update
  186.0 0.1 mul.240
  186.1 0.2 copy.43
  186.4 0.1 copy.45
  186.5 0.1 bitcast_reduce_fusion.1
  186.7 0.2 multiply_multiply_fusion
  186.9 0.2 subtract_convert_fusion
  187.1 0.0 all-gather.4.cloned.1.call-done
  187.1 2.7 fusion.48
  189.9 13.7 %bitcast_reduce_fusion = (f32[4,4,256]{2,1,0:T(4,128)S(1)}, f32[4,2048,256,4]{2,1,3,0:T(8,128)}) fusion(bf16[2048,4,64,1]{0,2,3,1:T(8,128)(2,1)S(1)} %bitcast.113, bf16[256,4,4,64]{0,3,2,1:T(8,128)(2,1)S(1)} %bitcast.114), kind=kOutput, calls=%fused_computation.4 | convolution fusion | flops 1090514944 | bytes 35143680 | tf_op jit(solution)/shard_map/tkgd,skd->kgts/dot_general | solution.py:49
  203.6 26.1 %all-gather.6.cloned.1.call-done = bf16[768,2048]{1,0:T(8,128)(2,1)} async-done(((bf16[768,512]{1,0:T(8,128)(2,1)}), bf16[768,2048]{1,0:T(8,128)(2,1)}) %all-gather.6.cloned.1.call-update) | async-done | bytes 3145744 | tf_op jit(solution)/shard_map/all_gather | solution.py:145
  229.7 6.6 %fusion.18 = bf16[1,768,1024]{2,1,0:T(8,128)(2,1)S(1)} fusion(bf16[768,2048]{1,0:T(8,128)(2,1)} %all-gather.6.cloned.1.call-done, bf16[1,2048,1024]{2,1,0:T(8,128)(2,1)} %param.23), kind=kOutput, calls=%fused_computation.24 | convolution fusion | flops 3222011904 | bytes 8912896 | tf_op jit(solution)/shard_map/erf,efd->erd/dot_general | solution.py:143
  236.2 2.4 copy.58
  238.7 0.5 broadcast.330
  239.2 11.2 %reduce.3 = bf16[768,1024]{1,0:T(8,128)(2,1)} reduce(bf16[768,1,1024]{2,1,0:T(2,128)(2,1)S(1)} %bitcast.108, bf16[]{:T(256)} %broadcast.330), dimensions={1}, to_apply=%bitcast.101.reduce_sub_computation | reduce | bytes 3145730
  250.4 4.1 %reshape.311 = bf16[8,2,49152]{2,1,0:T(2,128)(2,1)} reshape(bf16[768,1024]{1,0:T(8,128)(2,1)} %reduce.3) | data formatting | bytes 3145728
  254.5 4.6 %all-to-all-start.1 = ((bf16[8,2,49152]{2,1,0:T(2,128)(2,1)}), bf16[8,2,49152]{2,1,0:T(2,128)(2,1)S(1)}, u32[]{:S(2)}, u32[]{:S(2)}) async-start(bf16[8,2,49152]{2,1,0:T(2,128)(2,1)} %reshape.311), calls=%async_computation.1 | async-start | bytes 3145728 | tf_op jit(solution)/shard_map/all_to_all | solution.py:149
  259.1 13.6 %fusion.1 = f32[4,4,256]{2,1,0:T(4,128)S(1)} fusion(f32[4,2048,256,4]{2,1,3,0:T(8,128)} %get-tuple-element.19, f32[4,4,256]{2,1,0:T(4,128)S(1)} %get-tuple-element.18), kind=kLoop, calls=%fused_computation.6 | loop fusion | flops 25161728 | bytes 33587200 | tf_op jit(solution)/shard_map/reduce_sum | solution.py:55
  272.8 13.6 %fusion.34 = bf16[256,4,4,64]{0,3,2,1:T(8,128)(2,1)S(1)} fusion(bf16[2048,4,64,1]{0,2,3,1:T(8,128)(2,1)S(1)} %bitcast.112, f32[4,2048,256,4]{2,1,3,0:T(8,128)} %get-tuple-element.19, f32[4,4,256]{2,1,0:T(4,128)S(1)} %get-tuple-element.18, f32[256,4,4]{0,2,1:T(4,128)S(1)} %bitcast_add_fusion, f32[256,4,4]{0,2,1:T(4,128)S(1)} %multiply_bitcast_fusion), kind=kOutput, calls=%fused_computation.28 | convolution fusion | flops 1099694080 | bytes 35176448 | tf_op jit(solution)/shard_map/kgts,skd->kgtd/dot_general | solution.py:56
  286.4 1.0 copy.50
  287.4 9.5 %all-to-all-done.1 = bf16[8,2,49152]{2,1,0:T(2,128)(2,1)S(1)} async-done(((bf16[8,2,49152]{2,1,0:T(2,128)(2,1)}), bf16[8,2,49152]{2,1,0:T(2,128)(2,1)S(1)}, u32[]{:S(2)}, u32[]{:S(2)}) %all-to-all-start.1) | async-done | bytes 1572896 | tf_op jit(solution)/shard_map/all_to_all | solution.py:149
  296.9 3.9 %reshape.312 = bf16[768,1,1024]{2,1,0:T(2,128)(2,1)} reshape(bf16[8,2,49152]{2,1,0:T(2,128)(2,1)S(1)} %all-to-all-done.1) | data formatting | bytes 3145728
  300.8 2.5 copy.57
  303.3 2.1 gather_fusion.1
  305.4 1.3 reshape.278
  306.7 3.5 %multiply_reduce_fusion.1 = bf16[256,1024]{1,0:T(8,128)(2,1)} fusion(f32[256,2,1024]{2,1,0:T(2,128)S(1)} %reshape.278, f32[256,2]{1,0:T(8,128)S(1)} %copy.45), kind=kLoop, calls=%fused_computation.20 | loop fusion | flops 786432 | bytes 2623488 | tf_op jit(solution)/shard_map/reduce_sum | solution.py:153
  (40 shorter events, 0.4 us)
Async XLA Ops:
  7.2 180.0 %all-gather.4.cloned.1.call-start = ((), (), s32[]{:S(2)}) async-start(), calls=%async_computation.2 | async-start | bytes 2359296 | tf_op jit(solution)/shard_map/all_gather | solution.py:103
  14.4 119.4 %copy-start.2 = (bf16[256,256]{1,0:T(8,128)(2,1)S(1)}, bf16[256,256]{1,0:T(8,128)(2,1)}, u32[]{:S(2)}) copy-start(bf16[256,256]{1,0:T(8,128)(2,1)} %param.14) | copy-start | bytes 393220
  14.4 120.2 %copy-start.3 = (bf16[256,256]{1,0:T(8,128)(2,1)S(1)}, bf16[256,256]{1,0:T(8,128)(2,1)}, u32[]{:S(2)}) copy-start(bf16[256,256]{1,0:T(8,128)(2,1)} %param.13) | copy-start | bytes 393220
  61.2 36.7 %collective-permute-start = (bf16[1,768,1024]{2,1,0:T(8,128)(2,1)S(1)}, bf16[1,768,1024]{2,1,0:T(8,128)(2,1)S(1)}, u32[]{:S(2)}, u32[]{:S(2)}) collective-permute-start(bf16[1,768,1024]{2,1,0:T(8,128)(2,1)S(1)} %bitcast.105), channel_id=1, source_target_pairs={{0,1},{1,2},{2,3},{3,0},{4,5},{5,6},{6,7},{7,4},{8,9},{9,10},{10,1... | collective-permute-start | bytes 4718600 | tf_op jit(solution)/shard_map/ppermute | solution.py:16
  97.8 35.9 %collective-permute-start.1 = (bf16[1,768,1024]{2,1,0:T(8,128)(2,1)S(1)}, bf16[1,768,1024]{2,1,0:T(8,128)(2,1)}, u32[]{:S(2)}, u32[]{:S(2)}) collective-permute-start(bf16[1,768,1024]{2,1,0:T(8,128)(2,1)S(1)} %collective-permute-done), channel_id=1, source_target_pairs={{0,1},{1,2},{2,3},{3,0},{4,5},{5,6},{6,7},{7,4},{8,9},{9,10},{10,1... | collective-permute-start | bytes 4718600 | tf_op jit(solution)/shard_map/ppermute | solution.py:16
  133.8 35.3 %collective-permute-start.2 = (bf16[1,768,1024]{2,1,0:T(8,128)(2,1)}, bf16[1,768,1024]{2,1,0:T(8,128)(2,1)}, u32[]{:S(2)}, u32[]{:S(2)}) collective-permute-start(bf16[1,768,1024]{2,1,0:T(8,128)(2,1)} %collective-permute-done.1), channel_id=1, source_target_pairs={{0,1},{1,2},{2,3},{3,0},{4,5},{5,6},{6,7},{7,4},{8,9},{9,10},{10,1... | collective-permute-start | bytes 4718600 | tf_op jit(solution)/shard_map/ppermute | solution.py:16
  135.9 93.7 %all-gather.6.cloned.1.call-start = ((), (), s32[]{:S(2)}) async-start(), calls=%async_computation.3 | async-start | bytes 3932160 | tf_op jit(solution)/shard_map/all_gather | solution.py:145
  175.8 2.2 copy-start.7
  178.0 3.4 %copy-start.8 = (bf16[1,4096,512]{2,1,0:T(8,128)(2,1)S(1)}, bf16[1,4096,512]{2,1,0:T(8,128)(2,1)}, u32[]{:S(2)}) copy-start(bf16[1,4096,512]{2,1,0:T(8,128)(2,1)} %param.22) | copy-start | bytes 12582916
  181.4 4.6 %copy-start.6 = (f32[64]{0:T(128)S(1)}, f32[64]{0:T(128)}, u32[]{:S(2)}) copy-start(f32[64]{0:T(128)} %param.15) | copy-start | bytes 772
  181.4 4.7 %copy-start.1 = (bf16[256,1024]{1,0:T(8,128)(2,1)S(1)}, bf16[256,1024]{1,0:T(8,128)(2,1)}, u32[]{:S(2)}) copy-start(bf16[256,1024]{1,0:T(8,128)(2,1)} %param.12) | copy-start | bytes 1572868
  181.4 4.9 %copy-start.4 = (f32[256,2]{0,1:T(2,128)S(1)}, f32[256,2]{0,1:T(2,128)}, u32[]{:S(2)}) copy-start(f32[256,2]{0,1:T(2,128)} %param.20) | copy-start | bytes 6148
  181.5 4.9 %copy-start.5 = (f32[256]{0:T(256)S(1)}, f32[256]{0:T(256)}, u32[]{:S(2)}) copy-start(f32[256]{0:T(256)} %param.19) | copy-start | bytes 3076
  254.5 42.4 %all-to-all-start.1 = ((bf16[8,2,49152]{2,1,0:T(2,128)(2,1)}), bf16[8,2,49152]{2,1,0:T(2,128)(2,1)S(1)}, u32[]{:S(2)}, u32[]{:S(2)}) async-start(bf16[8,2,49152]{2,1,0:T(2,128)(2,1)} %reshape.311), calls=%async_computation.1 | async-start | bytes 3145728 | tf_op jit(solution)/shard_map/all_to_all | solution.py:149
  259.1 13.7 %copy-start = (bf16[2048,256]{0,1:T(8,128)(2,1)S(1)}, bf16[2048,256]{0,1:T(8,128)(2,1)}, u32[]{:S(2)}) copy-start(bf16[2048,256]{0,1:T(8,128)(2,1)} %get-tuple-element.11) | copy-start | bytes 3145732
Sparse Core Ops, SparseCore 0:
  136.0 31.2 all-gather.3
  186.1 43.4 all-gather.5
